TPU v7x, 256 devices: a whole 4x4x8 slice. The times are simulated.
256 devices in a mesh: dp: 4 (over x), kv: 32 (over z, y), tp: 2 (over core).
Axes of the slice: x: 4, y: 4, z: 8, core: 2. Of those that a mesh axis runs over, the one named last changes fastest.
Arguments:
- tokens: bfloat16 [512, 2048], P('dp', ('kv', 'tp')), may hold values from -30 to 30
- state: float32 [512, 4, 256, 512], P(('dp', 'kv'), 'tp'), may hold values from -6 to 6
- mix_gain: float32 [2048], P('kv'), may hold values from 0.1 to 1.9
- w_query: bfloat16 [2048, 1024], P('kv', 'tp'), may hold values from -0.125 to 0.125
- w_key: bfloat16 [2048, 1024], P('kv', 'tp'), may hold values from -0.125 to 0.125
- w_decay: bfloat16 [2048, 1024], P('kv', 'tp'), may hold values from -0.125 to 0.125
- w_value: bfloat16 [2048, 2048], P('kv', 'tp'), may hold values from -0.125 to 0.125
- w_gate: bfloat16 [2048, 2048], P('kv', 'tp'), may hold values from -0.125 to 0.125
- decay_offset: float32 [1024], P('tp'), may hold values from -1 to 4
- head_gain: float32 [512], replicated, may hold values from 0.1 to 1.9
- w_out: bfloat16 [2048, 2048], P('tp', 'kv'), may hold values from -0.125 to 0.125
- mlp_gain: float32 [2048], replicated, may hold values from 0.1 to 1.9
- w_up: bfloat16 [2048, 8192], P(None, ('kv', 'tp')), may hold values from -0.125 to 0.125
- w_down: bfloat16 [8192, 2048], P(('kv', 'tp')), may hold values from -0.1875 to 0.1875
Outputs:
- mixed: bfloat16 [512, 2048], P('dp', ('kv', 'tp'))
- new_state: float32 [512, 4, 256, 512], P(('dp', 'kv'), 'tp')
All inputs are finite; a program needn't handle non-finite values.
Results may differ from a plain program's by a relative error of at most 0.013.
Values may be sent and summed in bfloat16 or wider, within the bound.
A program may use at most 64 MiB of HBM per device.

v0:
```python
import jax
import jax.numpy as jnp
from jax import lax
from jax.sharding import PartitionSpec as P

D = 2048


epsilon = 1e-06


def laid_out(blocks, dim):
    dims = list(blocks.shape[1:])
    dims[dim] *= blocks.shape[0]
    return jnp.moveaxis(blocks, 0, dim).reshape(dims)


def copy_for_each(shard, axis):
    count = lax.axis_size(axis)
    return lax.all_to_all(
        jnp.broadcast_to(shard[None], (count, *shard.shape)), axis, 0, 0, tiled=True
    )


def collect(shard, axis, dim):
    return laid_out(copy_for_each(shard, axis), dim)


def in_blocks(shard, dim, count):
    before, after = (shard.shape[:dim], shard.shape[dim + 1 :])
    return jnp.moveaxis(shard.reshape(*before, count, -1, *after), dim, 0)


def summed_on_arrival(shard, axis, dim):
    count = lax.axis_size(axis)
    blocks = lax.all_to_all(in_blocks(shard, dim, count), axis, 0, 0, tiled=True)
    return jnp.sum(blocks.astype(jnp.float32), axis=0)


def in_one_piece(arrays, axis, dim, along):
    columns = [a.reshape(*a.shape[:along], -1) for a in arrays]
    both = jnp.concatenate(columns, axis=along)
    whole, at, outs = (summed_on_arrival(both, axis, dim), 0, [])
    for a, column in zip(arrays, columns):
        section = whole[..., at : at + column.shape[along]]
        outs.append(section.reshape(*section.shape[:along], *a.shape[along:]))
        at += column.shape[along]
    return tuple(outs)


def shards(
    tokens,
    state,
    mix_gain,
    w_query,
    w_key,
    w_decay,
    w_value,
    w_gate,
    decay_offset,
    head_gain,
    w_out,
    mlp_gain,
    w_up,
    w_down,
):
    seq_dev = state.shape[0]
    heads_here = state.shape[1]
    key_dim = state.shape[2]
    val_dim = state.shape[3]
    weights = (w_query, w_key, w_decay, w_value, w_gate)
    tok_cols = collect(tokens, "tp", 1)
    tok_float = tok_cols.astype(jnp.float32)
    squares = jnp.sum(tok_float * tok_float, axis=1)
    scaled = (tok_float * mix_gain).astype(jnp.bfloat16)
    projected, row_sums = in_one_piece(
        (
            jnp.concatenate(
                [jnp.dot(scaled, weight, preferred_element_type=jnp.float32) for weight in weights],
                axis=1,
            ).astype(jnp.bfloat16),
            squares.astype(jnp.bfloat16),
        ),
        "kv",
        0,
        1,
    )
    row_scale = lax.rsqrt(row_sums / D + epsilon)[:, None]
    projected = projected * row_scale
    key_width = heads_here * key_dim
    val_width = heads_here * val_dim
    queries = (projected[:, :key_width] * key_dim ** (-0.5)).reshape(seq_dev, heads_here, key_dim)
    new_keys = projected[:, key_width : 2 * key_width].reshape(seq_dev, heads_here, key_dim)
    retain = jax.nn.sigmoid(projected[:, 2 * key_width : 3 * key_width] + decay_offset).reshape(
        seq_dev, heads_here, key_dim
    )
    values = projected[:, 3 * key_width : 3 * key_width + val_width].reshape(
        seq_dev, heads_here, val_dim
    )
    gates = projected[:, 3 * key_width + val_width :]
    new_state = retain[..., None] * state + new_keys[..., None] * values[:, :, None, :]
    readout = jnp.einsum("bhk,bhkv->bhv", queries, new_state, precision=lax.Precision.HIGHEST)
    readout = (
        readout
        * lax.rsqrt(jnp.mean(readout * readout, axis=2, keepdims=True) + epsilon)
        * head_gain
    )
    gated = (readout.reshape(seq_dev, val_width) * jax.nn.silu(gates)).astype(jnp.bfloat16)
    branch = jnp.dot(collect(gated, "kv", 0), w_out, preferred_element_type=jnp.float32)
    branch_own = summed_on_arrival(branch.astype(jnp.bfloat16), "tp", 1)
    stream_own = (tokens.astype(jnp.float32) + branch_own).astype(jnp.bfloat16)
    stream = collect(stream_own, ("kv", "tp"), 1)
    stream_float = stream.astype(jnp.float32)
    mlp_scale = lax.rsqrt(jnp.mean(stream_float * stream_float, axis=1, keepdims=True) + epsilon)
    normed = (stream_float * mlp_gain).astype(jnp.bfloat16)
    hidden = jnp.dot(normed, w_up, preferred_element_type=jnp.float32) * mlp_scale
    squared = jnp.square(jax.nn.relu(hidden)).astype(jnp.bfloat16)
    down_own = summed_on_arrival(
        lax.dot_general(
            w_down, squared, (((0,), (1,)), ((), ())), preferred_element_type=jnp.float32
        ).astype(jnp.bfloat16),
        ("kv", "tp"),
        0,
    )
    mixed = (stream_own.astype(jnp.float32) + down_own.T).astype(jnp.bfloat16)
    return (mixed, new_state)


def solution(mesh):
    in_specs = (
        P("dp", ("kv", "tp")),
        P(("dp", "kv"), "tp", None, None),
        P("kv"),
        P("kv", "tp"),
        P("kv", "tp"),
        P("kv", "tp"),
        P("kv", "tp"),
        P("kv", "tp"),
        P("tp"),
        P(),
        P("tp", "kv"),
        P(),
        P(None, ("kv", "tp")),
        P(("kv", "tp"), None),
    )
    out_specs = (P("dp", ("kv", "tp")), P(("dp", "kv"), "tp", None, None))
    return jax.shard_map(shards, mesh=mesh, in_specs=in_specs, out_specs=out_specs, check_vma=False)
```

profile of v0, /device:TPU:1, one launch (start us, length us, event | category | flops | bytes accessed | tf_op | source)
XLA Modules:
  0.0 127.3 jit_solution(16025493795749854072)
XLA Ops:
  0.6 0.0 copy-start
  0.6 0.0 copy-start.6
  0.7 0.8 broadcast_in_dim.6
  1.4 6.6 %all_to_all.30 = bf16[2,128,32]{1,2,0:T(8,128)(2,1)S(1)} all-to-all(bf16[2,128,32]{1,2,0:T(8,128)(2,1)S(1)} %broadcast_in_dim.6), channel_id=1, replica_groups=mesh['dp'=4,'kv'=32,'tp'=2] {'tp'}, dimensions={0} | all-to-all | bytes 32768 | tf_op jit(solution)/shard_map/all_to_all | solution.py:20
  8.0 0.1 convert_element_type.101
  8.1 0.3 copy.57
  8.5 0.1 copy.55
  8.6 0.1 reshape.108
  8.8 0.7 fusion.15
  9.4 1.0 fusion.5
  10.4 1.0 fusion.4
  11.4 1.0 fusion.3
  12.5 1.1 fusion.2
  13.6 1.1 fusion.1
  14.7 0.5 copy.58
  15.2 33.8 %all_to_all.31 = bf16[32,4,3585]{2,1,0:T(4,128)(2,1)S(1)} all-to-all(bf16[32,4,3585]{2,1,0:T(4,128)(2,1)S(1)} %copy.58), channel_id=1, replica_groups=mesh['dp'=4,'kv'=32,'tp'=2] {'kv'}, dimensions={0} | all-to-all | bytes 1835520 | tf_op jit(solution)/shard_map/all_to_all | solution.py:36
  49.0 0.2 convert_reduce_fusion
  49.2 0.1 fusion.31
  49.3 0.1 slice_multiply_fusion
  49.4 0.0 copy-done.6
  49.5 2.6 %multiply_add_fusion = f32[4,2,256,512]{3,2,1,0:T(8,128)S(1)} fusion(f32[4,2,256,512]{3,2,1,0:T(8,128)} %param.15, f32[4,2,512]{2,1,0:T(2,128)S(1)} %mul.121, f32[4,2,256]{2,1,0:T(2,128)S(1)} %mul.119, f32[4,2,256]{2,1,0:T(2,128)S(1)} %mul.116), kind=kLoop, calls=%fused_computation | loop fusion | flops 3145728 | bytes 8421376 | tf_op jit(solution)/shard_map/add | solution.py:101
  52.1 0.0 copy-start.1
  52.1 2.0 %copy-done.1 = f32[4,2,256,512]{3,2,1,0:T(8,128)} copy-done((f32[4,2,256,512]{3,2,1,0:T(8,128)}, f32[4,2,256,512]{3,2,1,0:T(8,128)S(1)}, u32[]{:S(2)}) %copy-start.1) | copy-done | bytes 4194328
  54.1 0.0 copy-start.7
  54.1 0.0 copy-start.2
  54.2 2.1 %fusion.33 = f32[4,2,1,512]{3,2,1,0:T(1,128)S(1)} fusion(f32[4,2,256,1]{2,3,1,0:T(1,128)S(1)} %reshape.118, f32[4,2,256,512]{3,2,1,0:T(8,128)S(1)} %multiply_add_fusion), kind=kOutput, calls=%fused_computation.62 | convolution fusion | flops 12582912 | bytes 4218880 | tf_op jit(solution)/shard_map/bhk,bhkv->bhv/dot_general | solution.py:102
  56.2 0.1 fusion.21
  56.3 0.0 copy-done.7
  56.3 0.1 fusion.23
  56.5 0.1 broadcast_in_dim.7
  56.5 16.3 %all_to_all.32 = bf16[32,4,1024]{2,1,0:T(4,128)(2,1)S(1)} all-to-all(bf16[32,4,1024]{2,1,0:T(4,128)(2,1)S(1)} %broadcast_in_dim.7), channel_id=1, replica_groups=mesh['dp'=4,'kv'=32,'tp'=2] {'kv'}, dimensions={0} | all-to-all | bytes 524288 | tf_op jit(solution)/shard_map/all_to_all | solution.py:20
  72.8 0.1 reshape.105
  72.9 0.0 copy-done.3
  72.9 0.2 convolution_convert_fusion.6
  73.1 7.1 %all_to_all.33 = bf16[2,128,32]{1,2,0:T(8,128)(2,1)S(1)} all-to-all(bf16[2,128,32]{1,2,0:T(8,128)(2,1)S(1)} %bitcast.58), channel_id=1, replica_groups=mesh['dp'=4,'kv'=32,'tp'=2] {'tp'}, dimensions={0} | all-to-all | bytes 32768 | tf_op jit(solution)/shard_map/all_to_all | solution.py:36
  80.3 0.0 copy-done.4
  80.3 0.1 broadcast_in_dim.8
  80.4 21.6 %all_to_all.34 = bf16[64,128,32]{1,2,0:T(8,128)(2,1)S(1)} all-to-all(bf16[64,128,32]{1,2,0:T(8,128)(2,1)S(1)} %broadcast_in_dim.8), channel_id=1, replica_groups=mesh['dp'=4,'kv'=32,'tp'=2] {'kv','tp'}, dimensions={0} | all-to-all | bytes 1048576 | tf_op jit(solution)/shard_map/all_to_all | solution.py:20
  101.9 0.3 multiply_reduce_fusion
  102.2 0.0 copy-done.5
  102.2 0.3 fusion.9
  102.6 0.0 copy-done
  102.6 0.0 copy-done.2
  102.6 0.6 fusion
  103.2 0.3 copy.60
  103.5 23.2 %all_to_all.35 = bf16[64,32,128]{2,1,0:T(8,128)(2,1)S(1)} all-to-all(bf16[64,32,128]{2,1,0:T(8,128)(2,1)S(1)} %bitcast.57), channel_id=1, replica_groups=mesh['dp'=4,'kv'=32,'tp'=2] {'kv','tp'}, dimensions={0} | all-to-all | bytes 1048576 | tf_op jit(solution)/shard_map/all_to_all | solution.py:36
  126.6 0.1 convert_reduce_fusion.1
  126.7 0.6 fusion.20
  (18 shorter events, 0.2 us)
Async XLA Ops:
  0.6 101.9 %copy-start = (bf16[128,2048]{1,0:T(8,128)(2,1)S(1)}, bf16[128,2048]{1,0:T(8,128)(2,1)}, u32[]{:S(2)}) copy-start(bf16[128,2048]{1,0:T(8,128)(2,1)} %param.27) | copy-start | bytes 1572868
  0.6 48.8 %copy-start.6 = (f32[512]{0:T(512)S(1)}, f32[512]{0:T(512)}, u32[]{:S(2)}) copy-start(f32[512]{0:T(512)} %param.22) | copy-start | bytes 6148
  52.1 2.0 %copy-start.1 = (f32[4,2,256,512]{3,2,1,0:T(8,128)}, f32[4,2,256,512]{3,2,1,0:T(8,128)S(1)}, u32[]{:S(2)}) copy-start(f32[4,2,256,512]{3,2,1,0:T(8,128)S(1)} %multiply_add_fusion) | copy-start | bytes 12582916
  54.1 2.2 %copy-start.7 = (f32[512]{0:T(512)S(1)}, f32[512]{0:T(512)}, u32[]{:S(2)}) copy-start(f32[512]{0:T(512)} %param.23) | copy-start | bytes 6148
  54.1 18.8 %copy-start.3 = (bf16[1024,64]{0,1:T(8,128)(2,1)S(1)}, bf16[1024,64]{0,1:T(8,128)(2,1)}, u32[]{:S(2)}) copy-start(bf16[1024,64]{0,1:T(8,128)(2,1)} %param.24) | copy-start | bytes 393220
  54.1 26.1 %copy-start.4 = (bf16[128,32]{0,1:T(8,128)(2,1)S(1)}, bf16[128,32]{0,1:T(8,128)(2,1)}, u32[]{:S(2)}) copy-start(bf16[128,32]{0,1:T(8,128)(2,1)} %param.14) | copy-start | bytes 24580
  54.1 48.1 %copy-start.5 = (f32[2048]{0:T(1024)S(1)}, f32[2048]{0:T(1024)}, u32[]{:S(2)}) copy-start(f32[2048]{0:T(1024)} %param.25) | copy-start | bytes 24580
  54.1 48.4 %copy-start.2 = (bf16[2048,128]{1,0:T(8,128)(2,1)S(1)}, bf16[2048,128]{1,0:T(8,128)(2,1)}, u32[]{:S(2)}) copy-start(bf16[2048,128]{1,0:T(8,128)(2,1)} %param.26) | copy-start | bytes 1572868
where the time goes:
time: 128 us; the launch traced here: 127 us
  blocking collectives  109 us (85%)
  matrix products  8.08 us (6%)
  other arithmetic  5.26 us (4%)
  local copies, waits for them, and re-layouts  4.6 us (4%)
    all_to_all x3, blocking collectives, summed_on_arrival(): lax.all_to_all(in_blocks(shard, dim, count), axis, 0, 0, tiled=True)  64.1 us
    all_to_all x3, blocking collectives, copy_for_each(): lax.all_to_all(jnp.broadcast_to(shard[None], (count, *shard.shape)), axis...  44.4 us
    dot_general x5, matrix products, shards(): jnp.dot(scaled, weight, preferred_element_type=jnp.float32)  5.22 us
    add x1, other arithmetic, shards(): retain[..., None] * state + new_keys[..., None] * values[:, :, None, :]  2.59 us

commit v1 on v0

v1 whole, which is shorter than its diff:
```python
import jax
import jax.numpy as jnp
from jax import lax
from jax.experimental import pallas as pl
from jax.experimental.pallas import tpu as pltpu
from jax.sharding import PartitionSpec as P

MESH = pl.DeviceIdType.MESH
F32, BF16 = jnp.float32, jnp.bfloat16
D = 2048
EPS = 1e-06
NY, NZ = 4, 8
Q, K, R, S, V, G = (slice(0, 128), slice(128, 256), slice(256, 384), slice(384, 512), slice(512, 768), slice(768, 1024))
PIECES = ((V, (3,)), (G, (4,)), (slice(0, 256), (0, 1)), (slice(256, 512), (2,)))
COLUMNS = (Q, K, R, V, G)


def halves_side_by_side(top, bottom):
    lane = lax.broadcasted_iota(jnp.int32, top.shape, 1)
    return jnp.where(lane < 64, top, pltpu.roll(bottom, 64, 1))


def second_halves(top, bottom):
    lane = lax.broadcasted_iota(jnp.int32, top.shape, 1)
    return jnp.where(lane < 64, pltpu.roll(top, 64, 1), bottom)


def step(
    tok_h, state_h, gain_h, wq_h, wk_h, wd_h, wv_h, wg_h, off_h, hg_h, wo_h, mg_h, wu_h, wdn_h,
    mixed_ref, new_h,
    toks, pad, unit, gain, wq, wk, wd, wv, wg, off, hg, mg, wo, wu, wdn, state,
    xg, wgat, zs, zr, ys, yr, cols, vals, gs, gr, gf, sp, sr, xf, fs, fr, fz, zr6, mx,
    send_sem, recv_sem, local_sem, gr_sem,
):
    kv, t = lax.axis_index("kv"), lax.axis_index("tp")
    y, z = lax.rem(kv, NY), lax.div(kv, NY)
    other = 1 - t

    def at_y(dy):
        return lax.rem(y + dy + NY, NY)

    def at_z(dz):
        return lax.rem(z + dz + NZ, NZ)

    barrier = pltpu.get_barrier_semaphore()

    def greet(to_y, to_z, to_t):
        pl.semaphore_signal(
            barrier, inc=1, device_id={"kv": to_z * NY + to_y, "tp": to_t}, device_id_type=MESH
        )

    greet(y, z, other)
    for dy in range(1, NY):
        greet(at_y(dy), z, t)
        greet(at_y(dy), z, other)
    for dz in range(1, NZ):
        greet(y, at_z(dz), t)
        greet(y, at_z(dz), other)
    greetings = 1 + 2 * (NY - 1) + 2 * (NZ - 1)

    local = []

    def fetch(src, dst):
        copy = pltpu.make_async_copy(src, dst, local_sem.at[len(local)])
        copy.start()
        local.append(copy)
        return copy

    sends = []

    def send(src, dst, to_y, to_z, to_t, recv=None):
        n = len(sends)
        copy = pltpu.make_async_remote_copy(
            src_ref=src,
            dst_ref=dst,
            send_sem=send_sem.at[n],
            recv_sem=recv_sem.at[n] if recv is None else recv,
            device_id={"kv": to_z * NY + to_y, "tp": to_t},
            device_id_type=MESH,
        )
        copy.start()
        sends.append(copy)
        return copy

    tok_in = [fetch(tok_h, toks.at[t]), fetch(gain_h, gain)]
    weights, staged = (wq_h, wk_h, wd_h, wv_h, wg_h), (wq, wk, wd, wv, wg)
    weight_in, own_in = [None] * 5, [None] * 5
    for n in (3, 4, 0, 1, 2):
        weight_in[n] = fetch(weights[n], staged[n])
    for n in (3, 4, 0, 1, 2):
        width = COLUMNS[n].stop - COLUMNS[n].start
        mine = pl.ds(pl.multiple_of(y * width, width), width)
        own_in[n] = fetch(
            weights[n].at[:, mine], wgat.at[pl.ds(pl.multiple_of(y * 64, 64), 64), COLUMNS[n]]
        )
    half_lanes = pl.ds(pl.multiple_of(t * 128, 128), 128)
    half_rows = pl.ds(pl.multiple_of(t * 128, 128), 128)
    wo_in = fetch(wo_h, wo.at[t])
    wu_in = fetch(wu_h, wu.at[:, half_lanes])
    wdn_in = fetch(wdn_h, wdn.at[half_rows])
    small_in = [fetch(off_h, off), fetch(hg_h, hg), fetch(mg_h, mg)]
    state_in = fetch(state_h, state)

    for copy in tok_in:
        copy.wait()
    tok = toks[t].astype(F32)
    both_gains = gain[...]
    my_gain = jnp.where(t == 0, both_gains[:, :32], both_gains[:, 32:])
    pad[...] = jnp.zeros_like(pad)
    pad[:, 0:32] = (tok * my_gain).astype(BF16).astype(F32)
    pad[:, 32:64] = tok
    turned = pad[...].T
    squares = jnp.sum(turned[32:64] * turned[32:64], axis=0, keepdims=True)
    high = squares.astype(BF16).astype(F32)
    rows = lax.broadcasted_iota(jnp.int32, (16, 128), 0)
    sums = jnp.where(rows == 0, high, jnp.where(rows == 1, squares - high, 0.0))
    unit[0:32] = turned[0:32].astype(BF16)
    unit[32:48] = sums.astype(BF16)
    xg[y, t] = unit[...]
    for copy in weight_in:
        copy.wait()

    pl.semaphore_wait(barrier, greetings)

    x_in = [send(unit, xg.at[y, t], y, z, other)]
    for dy in range(1, NY):
        x_in.append(send(unit, xg.at[y, t], at_y(dy), z, t))
        x_in.append(send(unit, xg.at[y, t], at_y(dy), z, other))
    w_in = [[] for _ in range(5)]
    for n in (3, 4, 0, 1, 2):
        width = COLUMNS[n].stop - COLUMNS[n].start
        for dy in (2, 1, 3):
            theirs = pl.ds(pl.multiple_of(at_y(dy) * width, width), width)
            w_in[n].append(
                send(
                    staged[n].at[:, theirs],
                    wgat.at[pl.ds(pl.multiple_of(y * 64, 64), 64), COLUMNS[n]],
                    at_y(dy),
                    z,
                    t,
                )
            )
    wo_in.wait()
    wu_in.wait()
    wdn_in.wait()
    twin_in = [
        send(toks.at[t], toks.at[t], y, z, other),
        send(wo.at[t], wo.at[t], y, z, other),
        send(wu.at[:, half_lanes], wu.at[:, half_lanes], y, z, other),
        send(wdn.at[half_rows], wdn.at[half_rows], y, z, other),
    ]

    for copy in x_in:
        copy.wait_recv()
    blocks = [xg[a, b].astype(F32) for a in range(NY) for b in range(2)]
    x = jnp.concatenate([block[0:32] for block in blocks], axis=0).T.astype(BF16)
    row_squares = sum(block[32:33] + block[33:34] for block in blocks)
    spread = jnp.broadcast_to(row_squares, (128, 128)).T
    spread_high = spread.astype(BF16).astype(F32)
    lane = lax.broadcasted_iota(jnp.int32, (128, 128), 1)
    zs[:, S] = jnp.where(lane < 64, spread_high, spread - spread_high).astype(BF16)
    z_in = []
    for columns, members in PIECES:
        for n in members:
            own_in[n].wait()
            for copy in w_in[n]:
                copy.wait_recv()
        if members == (2,):
            zs[:, R] = jnp.dot(x, wgat[:, R], preferred_element_type=F32).astype(BF16)
        else:
            zs[:, columns] = jnp.dot(x, wgat[:, columns], preferred_element_type=F32).astype(BF16)
        z_in.append([])
        for dz in (4, 3, 5, 2, 6, 1, 7):
            theirs = pl.ds(pl.multiple_of(at_z(dz) * 16, 16), 16)
            z_in[-1].append(
                send(zs.at[theirs, columns], zr.at[z, :, columns], y, at_z(dz), t)
            )
    for (columns, members), copies in zip(PIECES, z_in):
        mine = pl.ds(pl.multiple_of(z * 16, 16), 16)
        total = zs[mine, columns].astype(F32)
        for copy in copies:
            copy.wait_recv()
        for dz in range(1, NZ):
            total = total + zr[at_z(dz), :, columns].astype(F32)
        for a in range(NY):
            ys[a, :, columns] = total[4 * a : 4 * a + 4]
    y_in = [send(ys.at[at_y(dy)], yr.at[y], at_y(dy), z, t) for dy in (2, 1, 3)]
    yr[y] = ys[y]
    for copy in small_in:
        copy.wait()
    state_in.wait()
    for copy in y_in:
        copy.wait_recv()

    got = [yr[a] for a in range(NY)]
    row_sum = got[0][:, 384:385] + got[0][:, 448:449]
    scale = lax.rsqrt(row_sum / D + EPS)
    queries = jnp.concatenate([g[:, Q] for g in got], axis=1) * scale * (256 ** -0.5)
    keys = jnp.concatenate([g[:, K] for g in got], axis=1) * scale
    retain = jax.nn.sigmoid(jnp.concatenate([g[:, R] for g in got], axis=1) * scale + off[...])
    cols[0:4] = queries
    cols[4:8] = keys
    cols[8:12] = retain
    cols[12:16] = jnp.zeros((4, 512), F32)
    upright = cols[...].T
    values = jnp.concatenate([g[:, V] for g in got], axis=1) * scale
    gates = jnp.concatenate([g[:, G] for g in got], axis=1) * scale
    silu = gates * jax.nn.sigmoid(gates)
    new_out = []
    for b in range(4):
        for h in range(2):
            value = values[b : b + 1, h * 512 : h * 512 + 512]
            total = jnp.zeros((8, 512), F32)
            for i in range(0, 256, 32):
                at = slice(h * 256 + i, h * 256 + i + 32)
                fresh = (
                    upright[at, 8 + b : 9 + b] * state[b, h, i : i + 32, :]
                    + upright[at, 4 + b : 5 + b] * value
                )
                state[b, h, i : i + 32, :] = fresh
                part = upright[at, b : b + 1] * fresh
                total = total + ((part[0:8] + part[8:16]) + (part[16:24] + part[24:32]))
            readout = jnp.sum(total, axis=0, keepdims=True)
            power = jnp.mean(readout * readout, axis=1, keepdims=True)
            vals[b : b + 1, h * 512 : h * 512 + 512] = (
                readout * lax.rsqrt(power + EPS) * hg[...]
            )
    gs[...] = (vals[...] * silu).astype(BF16)
    for b in range(4):
        new_out.append(fetch(state.at[b], new_h.at[b]))

    low = lax.rem(z, 4)
    home = lax.div(z, 4)
    for dz in range(1, NZ):
        send(gs, gr.at[y, low, t], y, at_z(dz), home, gr_sem.at[low, t])
    n = len(sends)

    @pl.when(home != t)
    def _():
        pltpu.make_async_remote_copy(
            src_ref=gs, dst_ref=gr.at[y, low, t], send_sem=send_sem.at[n], recv_sem=gr_sem.at[low, t],
            device_id={"kv": kv, "tp": other}, device_id_type=MESH,
        ).start()

    @pl.when(home == t)
    def _():
        gr[y, low, t] = gs[...]

    twin_gs = pltpu.make_async_copy(gs, gs, send_sem.at[n])
    sends.append(None)
    g_in = []
    for a in range(4):
        for c in range(2):
            @pl.when(jnp.logical_or(z != 4 * t + a, t != c))
            def _():
                pltpu.make_async_copy(gs, gr.at[y, a, c], gr_sem.at[a, c]).wait()
        g_in.append([send(gr.at[y, a], gr.at[y, a], at_y(dy), z, t) for dy in (2, 1, 3)])
    for copies in g_in:
        for copy in copies:
            copy.wait_recv()
    for a in range(4):
        for yy in range(NY):
            for c in range(2):
                gf[16 * a + 4 * yy : 16 * a + 4 * yy + 4, 1024 * c : 1024 * c + 1024] = gr[yy, a, c].astype(F32)

    for copy in twin_in:
        copy.wait_recv()
    branch = jnp.dot(gf[:, 0:1024].astype(BF16), wo[0], preferred_element_type=F32) + jnp.dot(
        gf[:, 1024:2048].astype(BF16), wo[1], preferred_element_type=F32
    )
    here = pl.ds(pl.multiple_of(t * 64, 64), 64)
    own_tok = jnp.concatenate([toks[0, here, :].astype(F32), toks[1, here, :].astype(F32)], axis=1)
    stream = (own_tok + branch).astype(BF16).astype(F32)
    packed = jnp.concatenate([stream[0:32], stream[32:64]], axis=1)
    sp[...] = packed.astype(BF16)
    s_in = {}
    for dz in (4, 3, 5, 2, 6, 1, 7):
        s_in[dz] = send(sp, sr.at[z, y], y, at_z(dz), t)
    sr[z, y] = sp[...]
    s_y = {}
    for dz in (0, 1, 7, 2, 6, 3, 5, 4):
        if dz:
            s_in[dz].wait_recv()
        src = at_z(-dz)
        s_y[dz] = [send(sr.at[src, y], sr.at[src, y], at_y(dy), z, t) for dy in (2, 1, 3)]
    hidden = jnp.zeros((64, 256), F32)
    power = jnp.zeros((64, 256), F32)
    for dz in (0, 1, 7, 2, 6, 3, 5, 4):
        src = at_z(-dz)
        for copy in s_y[dz]:
            copy.wait_recv()
        for p in range(2):
            a, b = sr[src, 2 * p].astype(F32), sr[src, 2 * p + 1].astype(F32)
            xf[0:32, 128 * p : 128 * p + 128] = halves_side_by_side(a, b)
            xf[32:64, 128 * p : 128 * p + 128] = second_halves(a, b)
        block = xf[...]
        power = power + block * block
        gain_here = mg[:, pl.ds(pl.multiple_of(src * 256, 256), 256)]
        hidden = hidden + jnp.dot(
            (block * gain_here).astype(BF16),
            wu[pl.ds(pl.multiple_of(src * 256, 256), 256), :],
            preferred_element_type=F32,
        )
    mlp_scale = lax.rsqrt(jnp.sum(power, axis=1, keepdims=True) / D + EPS)
    squared = jnp.square(jnp.maximum(hidden * mlp_scale, 0.0)).astype(BF16)

    order = (4, 3, 5, 2, 6, 1, 7, 0)
    d_in = {}
    for dz in order:
        theirs = pl.ds(pl.multiple_of(at_z(dz) * 256, 256), 256)
        part = jnp.dot(squared, wdn[:, theirs], preferred_element_type=F32)
        for p in range(2):
            top, bottom = part[0:32, 128 * p : 128 * p + 128], part[32:64, 128 * p : 128 * p + 128]
            fs[dz, 2 * p] = halves_side_by_side(top, bottom).astype(BF16)
            fs[dz, 2 * p + 1] = second_halves(top, bottom).astype(BF16)
        d_in[dz] = [send(fs.at[dz, at_y(dy)], fr.at[dz, dy], at_y(dy), z, t) for dy in (2, 1, 3)]
    e_in = []
    for dz in order:
        for copy in d_in[dz]:
            copy.wait_recv()
        total = fs[dz, y].astype(F32)
        for dy in range(1, NY):
            total = total + fr[dz, dy].astype(F32)
        if dz:
            fz[dz] = total.astype(BF16)
            e_in.append(send(fz.at[dz], zr6.at[dz], y, at_z(dz), t))
    for copy in e_in:
        copy.wait_recv()
    for dz in range(1, NZ):
        total = total + zr6[dz].astype(F32)
    mx[t] = (packed + total).astype(BF16)
    m_in = send(mx.at[t], mx.at[t], y, z, other)
    m_in.wait_recv()
    for c in range(2):
        block = mx[c].astype(F32)
        for h in range(2):
            quarter = jnp.where(
                t == 0, block[:, h * 64 : h * 64 + 32], block[:, h * 64 + 32 : h * 64 + 64]
            )
            mixed_ref[c * 64 + h * 32 : c * 64 + h * 32 + 32, :] = quarter.astype(BF16)

    for copy in sends:
        if copy is not None:
            copy.wait_send()

    @pl.when(home != t)
    def _():
        twin_gs.wait()

    for copy in new_out:
        copy.wait()


SENDS = 7 + 15 + 4 + 28 + 3 + 8 + 12 + 7 + 24 + 24 + 7 + 1


def shards(tokens, state, mix_gain, w_query, w_key, w_decay, w_value, w_gate, decay_offset, head_gain, w_out, mlp_gain, w_up, w_down):
    anywhere = pl.BlockSpec(memory_space=pl.ANY)
    vmem = pltpu.VMEM
    mixed, new_state = pl.pallas_call(
        step,
        out_shape=(
            jax.ShapeDtypeStruct(tokens.shape, BF16),
            jax.ShapeDtypeStruct(state.shape, F32),
        ),
        in_specs=[anywhere] * 14,
        out_specs=(pl.BlockSpec(memory_space=pltpu.VMEM), anywhere),
        scratch_shapes=[
            vmem((2, 128, 32), BF16),
            vmem((128, 128), F32),
            vmem((48, 128), BF16),
            vmem((1, 64), F32),
            vmem((64, 512), BF16),
            vmem((64, 512), BF16),
            vmem((64, 512), BF16),
            vmem((64, 1024), BF16),
            vmem((64, 1024), BF16),
            vmem((1, 512), F32),
            vmem((1, 512), F32),
            vmem((1, 2048), F32),
            vmem((2, 1024, 64), BF16),
            vmem((2048, 256), BF16),
            vmem((256, 2048), BF16),
            vmem((4, 2, 256, 512), F32),
            vmem((4, 2, 48, 128), BF16),
            vmem((256, 1024), BF16),
            vmem((128, 1024), BF16),
            vmem((8, 16, 1024), BF16),
            vmem((4, 4, 1024), F32),
            vmem((4, 4, 1024), F32),
            vmem((16, 512), F32),
            vmem((4, 1024), F32),
            vmem((4, 1024), BF16),
            vmem((4, 4, 2, 4, 1024), BF16),
            vmem((64, 2048), F32),
            vmem((32, 128), BF16),
            vmem((8, 4, 32, 128), BF16),
            vmem((64, 256), F32),
            vmem((8, 4, 32, 128), BF16),
            vmem((8, 4, 32, 128), BF16),
            vmem((8, 32, 128), BF16),
            vmem((8, 32, 128), BF16),
            vmem((2, 32, 128), BF16),
            pltpu.SemaphoreType.DMA((SENDS,)),
            pltpu.SemaphoreType.DMA((SENDS,)),
            pltpu.SemaphoreType.DMA((32,)),
            pltpu.SemaphoreType.DMA((4, 2)),
        ],
        compiler_params=pltpu.CompilerParams(
            collective_id=0, has_side_effects=True, vmem_limit_bytes=48 * 1024 * 1024
        ),
        name="layer_step",
    )(
        tokens, state, mix_gain.reshape(1, -1), w_query, w_key, w_decay, w_value, w_gate,
        decay_offset.reshape(1, -1), head_gain.reshape(1, -1), w_out, mlp_gain.reshape(1, -1), w_up, w_down,
    )
    return mixed, new_state


def solution(mesh):
    in_specs = (
        P("dp", ("kv", "tp")),
        P(("dp", "kv"), "tp", None, None),
        P("kv"),
        P("kv", "tp"),
        P("kv", "tp"),
        P("kv", "tp"),
        P("kv", "tp"),
        P("kv", "tp"),
        P("tp"),
        P(),
        P("tp", "kv"),
        P(),
        P(None, ("kv", "tp")),
        P(("kv", "tp"), None),
    )
    out_specs = (P("dp", ("kv", "tp")), P(("dp", "kv"), "tp", None, None))
    return jax.shard_map(shards, mesh=mesh, in_specs=in_specs, out_specs=out_specs, check_vma=False)
```

time: 128 us -> 79.5 us (0.62)
  blocking collectives: 109 us -> 0 us
  Pallas kernels: 0 us -> 60 us
  local copies, waits for them, and re-layouts: 4.6 us -> 18.3 us
  matrix products: 8.08 us -> 0 us
  other arithmetic: 5.26 us -> 0 us
    all_to_all x6 -> x0, blocking collectives: 109 us -> none  [the longest x3 64.1 us: summed_on_arrival(): lax.all_to_all(in_blocks(shard, dim, count), axis, 0, 0, tiled=True)]
    pallas_call x0 -> x1, Pallas kernels: none -> 60 us  [shards(): pl.pallas_call(step, out_shape=(jax.ShapeDtypeStruct(tokens.shape, BF16),...]
    unnamed x17 -> x27, local copies, waits for them, and re-layouts: 2.05 us -> 17.6 us
    dot_general x8 -> x0, matrix products: 8.08 us -> none  [the longest x5 5.22 us: shards(): jnp.dot(scaled, weight, preferred_element_type=jnp.float32)]
    add x1 -> x0, other arithmetic: 2.59 us -> none  [shards(): retain[..., None] * state + new_keys[..., None] * values[:, :, None, :]]
    convert_element_type x6 -> x0, other arithmetic: 1.65 us -> none  [the longest x1 0.67 us: shards(): scaled = (tok_float * mix_gain).astype(jnp.bfloat16)]
where the time goes in v1:
time: 79.5 us; the launch traced here: 78.9 us
  Pallas kernels  60 us (75%)
  local copies, waits for them, and re-layouts  18.3 us (23%)
    pallas_call x1, Pallas kernels, shards(): pl.pallas_call(step, out_shape=(jax.ShapeDtypeStruct(tokens.shape, BF16),...  60 us
    unnamed x27, local copies, waits for them, and re-layouts  17.6 us

profile of v1, /device:TPU:1, one launch (start us, length us, event | category | flops | bytes accessed | tf_op | source)
XLA Modules:
  0.0 78.9 jit_solution(1792444347246738832)
XLA Ops:
  0.6 0.8 %copy.16.tok_h = bf16[128,32]{1,0:T(8,128)(2,1)S(1)} copy(bf16[128,32]{0,1:T(8,128)(2,1)} %param.14) | data formatting | bytes 16384 | tf_op args[0]
  1.4 1.1 %copy.17.wo_h = bf16[1024,64]{1,0:T(8,128)(2,1)S(1)} copy(bf16[1024,64]{0,1:T(8,128)(2,1)} %param.24) | data formatting | bytes 262144 | tf_op args[10]
  2.5 0.0 copy-start.1
  2.5 1.0 %copy-done.1 = bf16[2048,128]{1,0:T(8,128)(2,1)S(1)} copy-done((bf16[2048,128]{1,0:T(8,128)(2,1)S(1)}, bf16[2048,128]{1,0:T(8,128)(2,1)}, u32[]{:S(2)}) %copy-start.1) | copy-done | bytes 524312
  3.6 0.0 copy-start.2
  3.6 1.0 %copy-done.2 = bf16[128,2048]{1,0:T(8,128)(2,1)S(1)} copy-done((bf16[128,2048]{1,0:T(8,128)(2,1)S(1)}, bf16[128,2048]{1,0:T(8,128)(2,1)}, u32[]{:S(2)}) %copy-start.2) | copy-done | bytes 524312
  4.6 0.0 copy-start.3
  4.6 0.9 %copy-done.3 = bf16[64,1024]{1,0:T(8,128)(2,1)S(1)} copy-done((bf16[64,1024]{1,0:T(8,128)(2,1)S(1)}, bf16[64,1024]{1,0:T(8,128)(2,1)}, u32[]{:S(2)}) %copy-start.3) | copy-done | bytes 131096
  5.5 0.0 copy-start.4
  5.5 0.9 %copy-done.4 = bf16[64,1024]{1,0:T(8,128)(2,1)S(1)} copy-done((bf16[64,1024]{1,0:T(8,128)(2,1)S(1)}, bf16[64,1024]{1,0:T(8,128)(2,1)}, u32[]{:S(2)}) %copy-start.4) | copy-done | bytes 131096
  6.4 0.0 copy-start.5
  6.4 0.8 %copy-done.5 = bf16[64,512]{1,0:T(8,128)(2,1)S(1)} copy-done((bf16[64,512]{1,0:T(8,128)(2,1)S(1)}, bf16[64,512]{1,0:T(8,128)(2,1)}, u32[]{:S(2)}) %copy-start.5) | copy-done | bytes 65560
  7.3 0.0 copy-start.6
  7.3 0.8 %copy-done.6 = bf16[64,512]{1,0:T(8,128)(2,1)S(1)} copy-done((bf16[64,512]{1,0:T(8,128)(2,1)S(1)}, bf16[64,512]{1,0:T(8,128)(2,1)}, u32[]{:S(2)}) %copy-start.6) | copy-done | bytes 65560
  8.1 0.0 copy-start.7
  8.1 0.8 %copy-done.7 = bf16[64,512]{1,0:T(8,128)(2,1)S(1)} copy-done((bf16[64,512]{1,0:T(8,128)(2,1)S(1)}, bf16[64,512]{1,0:T(8,128)(2,1)}, u32[]{:S(2)}) %copy-start.7) | copy-done | bytes 65560
  8.9 0.0 copy-start.8
  8.9 0.7 copy-done.8
  9.6 0.0 copy-start.9
  9.6 0.7 copy-done.9
  10.3 0.0 copy-start.10
  10.3 0.7 copy-done.10
  11.0 0.0 copy-start.11
  11.0 0.7 copy-done.11
  11.7 60.0 %layer_step.1 = (bf16[128,32]{1,0:T(8,128)(2,1)S(1)}, f32[4,2,256,512]{3,2,1,0:T(8,128)S(1)}) custom-call(bf16[128,32]{1,0:T(8,128)(2,1)S(1)} %copy.16.tok_h, f32[4,2,256,512]{3,2,1,0:T(8,128)} %state_h.1, f32[1,64]{1,0:T(1,128)S(1)} %bitcast.7, bf16[64,512]{1,0:T(8,128)(2,1)S(1)} %copy-done.5, bf16[64,512]{1,0:T(8,128)(2,1)S(1)} %copy-done.6, ...), custom_call_target="tpu_custom_call" | custom-call | tf_op jit(solution)/shard_map/layer_step/pallas_call | solution.py:360
  71.7 0.0 copy-start
  71.7 1.9 %copy-done = f32[4,2,256,512]{3,2,1,0:T(8,128)} copy-done((f32[4,2,256,512]{3,2,1,0:T(8,128)}, f32[4,2,256,512]{3,2,1,0:T(8,128)S(1)}, u32[]{:S(2)}) %copy-start) | copy-done | bytes 4194328
  73.6 0.7 copy.18
  74.3 4.6 %copy.20 = f32[4,2,256,512]{3,2,1,0:T(8,128)} copy(f32[4,2,256,512]{3,2,1,0:T(8,128)} %copy-done) | data formatting | bytes 8388608
Async XLA Ops:
  2.5 1.0 %copy-start.1 = (bf16[2048,128]{1,0:T(8,128)(2,1)S(1)}, bf16[2048,128]{1,0:T(8,128)(2,1)}, u32[]{:S(2)}) copy-start(bf16[2048,128]{1,0:T(8,128)(2,1)} %wu_h.1) | copy-start | bytes 1572868
  3.6 1.0 %copy-start.2 = (bf16[128,2048]{1,0:T(8,128)(2,1)S(1)}, bf16[128,2048]{1,0:T(8,128)(2,1)}, u32[]{:S(2)}) copy-start(bf16[128,2048]{1,0:T(8,128)(2,1)} %wdn_h.1) | copy-start | bytes 1572868
  4.6 0.9 %copy-start.3 = (bf16[64,1024]{1,0:T(8,128)(2,1)S(1)}, bf16[64,1024]{1,0:T(8,128)(2,1)}, u32[]{:S(2)}) copy-start(bf16[64,1024]{1,0:T(8,128)(2,1)} %wv_h.1) | copy-start | bytes 393220
  5.5 0.9 %copy-start.4 = (bf16[64,1024]{1,0:T(8,128)(2,1)S(1)}, bf16[64,1024]{1,0:T(8,128)(2,1)}, u32[]{:S(2)}) copy-start(bf16[64,1024]{1,0:T(8,128)(2,1)} %wg_h.1) | copy-start | bytes 393220
  6.4 0.8 %copy-start.5 = (bf16[64,512]{1,0:T(8,128)(2,1)S(1)}, bf16[64,512]{1,0:T(8,128)(2,1)}, u32[]{:S(2)}) copy-start(bf16[64,512]{1,0:T(8,128)(2,1)} %wq_h.1) | copy-start | bytes 196612
  7.3 0.8 %copy-start.6 = (bf16[64,512]{1,0:T(8,128)(2,1)S(1)}, bf16[64,512]{1,0:T(8,128)(2,1)}, u32[]{:S(2)}) copy-start(bf16[64,512]{1,0:T(8,128)(2,1)} %wk_h.1) | copy-start | bytes 196612
  8.1 0.8 %copy-start.7 = (bf16[64,512]{1,0:T(8,128)(2,1)S(1)}, bf16[64,512]{1,0:T(8,128)(2,1)}, u32[]{:S(2)}) copy-start(bf16[64,512]{1,0:T(8,128)(2,1)} %wd_h.1) | copy-start | bytes 196612
  8.9 0.7 copy-start.8
  9.6 0.7 copy-start.9
  10.3 0.7 copy-start.10
  11.0 0.7 copy-start.11
  71.7 2.0 %copy-start = (f32[4,2,256,512]{3,2,1,0:T(8,128)}, f32[4,2,256,512]{3,2,1,0:T(8,128)S(1)}, u32[]{:S(2)}) copy-start(f32[4,2,256,512]{3,2,1,0:T(8,128)S(1)} %get-tuple-element.7) | copy-start | bytes 12582916

commit v2 on v1

--- a/solution.py
+++ b/solution.py
@@ -27,8 +27,8 @@
 
 def step(
     tok_h, state_h, gain_h, wq_h, wk_h, wd_h, wv_h, wg_h, off_h, hg_h, wo_h, mg_h, wu_h, wdn_h,
-    mixed_ref, new_h,
-    toks, pad, unit, gain, wq, wk, wd, wv, wg, off, hg, mg, wo, wu, wdn, state,
+    mixed_ref, state,
+    toks, unit, gain, wq, wk, wd, wv, wg, off, hg, mg, wo, wu, wdn,
     xg, wgat, zs, zr, ys, yr, cols, vals, gs, gr, gf, sp, sr, xf, fs, fr, fz, zr6, mx,
     send_sem, recv_sem, local_sem, gr_sem,
 ):
@@ -104,17 +104,13 @@
     for copy in tok_in:
         copy.wait()
     tok = toks[t].astype(F32)
-    both_gains = gain[...]
-    my_gain = jnp.where(t == 0, both_gains[:, :32], both_gains[:, 32:])
-    pad[...] = jnp.zeros_like(pad)
-    pad[:, 0:32] = (tok * my_gain).astype(BF16).astype(F32)
-    pad[:, 32:64] = tok
-    turned = pad[...].T
-    squares = jnp.sum(turned[32:64] * turned[32:64], axis=0, keepdims=True)
+    both_gains = jnp.broadcast_to(gain[...], (128, 64)).T
+    my_gain = jnp.where(t == 0, both_gains[:32], both_gains[32:])
+    squares = jnp.sum(tok * tok, axis=0, keepdims=True)
     high = squares.astype(BF16).astype(F32)
     rows = lax.broadcasted_iota(jnp.int32, (16, 128), 0)
     sums = jnp.where(rows == 0, high, jnp.where(rows == 1, squares - high, 0.0))
-    unit[0:32] = turned[0:32].astype(BF16)
+    unit[0:32] = (tok * my_gain).astype(BF16)
     unit[32:48] = sums.astype(BF16)
     xg[y, t] = unit[...]
     for copy in weight_in:
@@ -206,7 +202,6 @@
     values = jnp.concatenate([g[:, V] for g in got], axis=1) * scale
     gates = jnp.concatenate([g[:, G] for g in got], axis=1) * scale
     silu = gates * jax.nn.sigmoid(gates)
-    new_out = []
     for b in range(4):
         for h in range(2):
             value = values[b : b + 1, h * 512 : h * 512 + 512]
@@ -226,8 +221,6 @@
                 readout * lax.rsqrt(power + EPS) * hg[...]
             )
     gs[...] = (vals[...] * silu).astype(BF16)
-    for b in range(4):
-        new_out.append(fetch(state.at[b], new_h.at[b]))
 
     low = lax.rem(z, 4)
     home = lax.div(z, 4)
@@ -265,11 +258,12 @@
 
     for copy in twin_in:
         copy.wait_recv()
-    branch = jnp.dot(gf[:, 0:1024].astype(BF16), wo[0], preferred_element_type=F32) + jnp.dot(
-        gf[:, 1024:2048].astype(BF16), wo[1], preferred_element_type=F32
-    )
-    here = pl.ds(pl.multiple_of(t * 64, 64), 64)
-    own_tok = jnp.concatenate([toks[0, here, :].astype(F32), toks[1, here, :].astype(F32)], axis=1)
+    rows_of = (((1,), (1,)), ((), ()))
+    branch = lax.dot_general(
+        gf[:, 0:1024].astype(BF16), wo[0], rows_of, preferred_element_type=F32
+    ) + lax.dot_general(gf[:, 1024:2048].astype(BF16), wo[1], rows_of, preferred_element_type=F32)
+    both_tok = jnp.concatenate([toks[0].astype(F32), toks[1].astype(F32)], axis=0).T
+    own_tok = jnp.where(t == 0, both_tok[0:64], both_tok[64:128])
     stream = (own_tok + branch).astype(BF16).astype(F32)
     packed = jnp.concatenate([stream[0:32], stream[32:64]], axis=1)
     sp[...] = packed.astype(BF16)
@@ -331,13 +325,12 @@
     mx[t] = (packed + total).astype(BF16)
     m_in = send(mx.at[t], mx.at[t], y, z, other)
     m_in.wait_recv()
+    quarters = []
     for c in range(2):
         block = mx[c].astype(F32)
-        for h in range(2):
-            quarter = jnp.where(
-                t == 0, block[:, h * 64 : h * 64 + 32], block[:, h * 64 + 32 : h * 64 + 64]
-            )
-            mixed_ref[c * 64 + h * 32 : c * 64 + h * 32 + 32, :] = quarter.astype(BF16)
+        quarters += [block, pltpu.roll(block, 64, 1)]
+    upright = jnp.concatenate(quarters, axis=0).T
+    mixed_ref[...] = jnp.where(t == 0, upright[0:32], upright[32:64]).astype(BF16)
 
     for copy in sends:
         if copy is not None:
@@ -347,7 +340,13 @@
     def _():
         twin_gs.wait()
 
-    for copy in new_out:
+
+def handed_on(mixed_in, new_in, mixed_ref, new_ref, sem):
+    copies = [pltpu.make_async_copy(new_in.at[b], new_ref.at[b], sem.at[b]) for b in range(4)]
+    copies.append(pltpu.make_async_copy(mixed_in, mixed_ref, sem.at[4]))
+    for copy in copies:
+        copy.start()
+    for copy in copies:
         copy.wait()
 
 
@@ -355,19 +354,19 @@
 
 
 def shards(tokens, state, mix_gain, w_query, w_key, w_decay, w_value, w_gate, decay_offset, head_gain, w_out, mlp_gain, w_up, w_down):
-    anywhere = pl.BlockSpec(memory_space=pl.ANY)
+    anywhere = pl.BlockSpec(memory_space=pltpu.HBM)
+    inside = pl.BlockSpec(memory_space=pltpu.VMEM)
     vmem = pltpu.VMEM
     mixed, new_state = pl.pallas_call(
         step,
         out_shape=(
-            jax.ShapeDtypeStruct(tokens.shape, BF16),
-            jax.ShapeDtypeStruct(state.shape, F32),
+            vmem(tokens.shape[::-1], BF16),
+            vmem(state.shape, F32),
         ),
         in_specs=[anywhere] * 14,
-        out_specs=(pl.BlockSpec(memory_space=pltpu.VMEM), anywhere),
+        out_specs=(inside, inside),
         scratch_shapes=[
-            vmem((2, 128, 32), BF16),
-            vmem((128, 128), F32),
+            vmem((2, 32, 128), BF16),
             vmem((48, 128), BF16),
             vmem((1, 64), F32),
             vmem((64, 512), BF16),
@@ -378,10 +377,9 @@
             vmem((1, 512), F32),
             vmem((1, 512), F32),
             vmem((1, 2048), F32),
-            vmem((2, 1024, 64), BF16),
+            vmem((2, 64, 1024), BF16),
             vmem((2048, 256), BF16),
             vmem((256, 2048), BF16),
-            vmem((4, 2, 256, 512), F32),
             vmem((4, 2, 48, 128), BF16),
             vmem((256, 1024), BF16),
             vmem((128, 1024), BF16),
@@ -407,14 +405,26 @@
             pltpu.SemaphoreType.DMA((4, 2)),
         ],
         compiler_params=pltpu.CompilerParams(
-            collective_id=0, has_side_effects=True, vmem_limit_bytes=48 * 1024 * 1024
+            collective_id=0, has_side_effects=True, vmem_limit_bytes=62_500_000
         ),
         name="layer_step",
     )(
-        tokens, state, mix_gain.reshape(1, -1), w_query, w_key, w_decay, w_value, w_gate,
-        decay_offset.reshape(1, -1), head_gain.reshape(1, -1), w_out, mlp_gain.reshape(1, -1), w_up, w_down,
+        tokens.T, state, mix_gain.reshape(1, -1), w_query, w_key, w_decay, w_value, w_gate,
+        decay_offset.reshape(1, -1), head_gain.reshape(1, -1), w_out.T, mlp_gain.reshape(1, -1), w_up, w_down,
     )
-    return mixed, new_state
+    mixed, new_state = pl.pallas_call(
+        handed_on,
+        out_shape=(
+            jax.ShapeDtypeStruct(mixed.shape, BF16),
+            jax.ShapeDtypeStruct(state.shape, F32),
+        ),
+        in_specs=[inside] * 2,
+        out_specs=(anywhere, anywhere),
+        scratch_shapes=[pltpu.SemaphoreType.DMA((5,))],
+        compiler_params=pltpu.CompilerParams(vmem_limit_bytes=1024 * 1024),
+        name="handed_on",
+    )(mixed, new_state)
+    return mixed.T, new_state
 
 
 def solution(mesh):

time: 79.5 us -> 62.4 us (0.78)
  local copies, waits for them, and re-layouts: 18.3 us -> 0 us
  Pallas kernels: 60 us -> 61.6 us
    unnamed x27 -> x0, local copies, waits for them, and re-layouts: 17.6 us -> none
    pallas_call x1 -> x2, Pallas kernels: 60 us -> 61.6 us  [the longest x1 59.6 us: shards(): pl.pallas_call(step, out_shape=(vmem(tokens.shape[::-1], BF16), vmem(stat...]
where the time goes in v2:
time: 62.4 us; the launch traced here: 62.3 us
  Pallas kernels  61.6 us (99%)
  between operations  0.64 us (1%)
    pallas_call x1, Pallas kernels, shards(): pl.pallas_call(step, out_shape=(vmem(tokens.shape[::-1], BF16), vmem(stat...  59.6 us
    pallas_call x1, Pallas kernels, shards(): pl.pallas_call(handed_on, out_shape=(jax.ShapeDtypeStruct(mixed.shape, BF...  2.05 us

profile of v2, /device:TPU:1, one launch (start us, length us, event | category | flops | bytes accessed | tf_op | source)
XLA Modules:
  0.0 62.3 jit_solution(11317884037449734620)
XLA Ops:
  0.6 59.6 %layer_step.1 = (bf16[32,128]{1,0:T(8,128)(2,1)S(1)}, f32[4,2,256,512]{3,2,1,0:T(8,128)S(1)}) custom-call(bf16[32,128]{1,0:T(8,128)(2,1)} %bitcast.8, f32[4,2,256,512]{3,2,1,0:T(8,128)} %state_h.1, f32[1,64]{1,0:T(1,128)} %bitcast.12, bf16[64,512]{1,0:T(8,128)(2,1)} %wq_h.1, bf16[64,512]{1,0:T(8,128)(2,1)} %wk_h.1, bf16[64,512]{1,0:T(8,128)(2,1)} %wd_h.1, ...), custom_call_target="tpu_custom_call" | custom-call | tf_op jit(solution)/shard_map/layer_step/pallas_call | solution.py:360
  60.2 2.1 %handed_on.1 = (bf16[32,128]{1,0:T(8,128)(2,1)}, f32[4,2,256,512]{3,2,1,0:T(8,128)}) custom-call(bf16[32,128]{1,0:T(8,128)(2,1)S(1)} %get-tuple-element.6.mixed_in, f32[4,2,256,512]{3,2,1,0:T(8,128)S(1)} %get-tuple-element.7.new_in), custom_call_target="tpu_custom_call" | custom-call | tf_op jit(solution)/shard_map/handed_on/pallas_call | solution.py:415

commit v3 on v2

v3 whole, which is shorter than its diff:
```python
import jax
import jax.numpy as jnp
from jax import lax
from jax.experimental import pallas as pl
from jax.experimental.pallas import tpu as pltpu
from jax.sharding import PartitionSpec as P

MESH = pl.DeviceIdType.MESH
F32, BF16 = jnp.float32, jnp.bfloat16
D = 2048
EPS = 1e-06
NX, NY, NZ = 4, 4, 8
Q, K, R, S, V, G = (slice(0, 128), slice(128, 256), slice(256, 384), slice(384, 512), slice(512, 768), slice(768, 1024))
PIECES = ((V, (3,)), (G, (4,)), (slice(0, 256), (0, 1)), (slice(256, 512), (2,)))
COLUMNS = (Q, K, R, V, G)


def halves_side_by_side(top, bottom):
    lane = lax.broadcasted_iota(jnp.int32, top.shape, 1)
    return jnp.where(lane < 64, top, pltpu.roll(bottom, 64, 1))


def second_halves(top, bottom):
    lane = lax.broadcasted_iota(jnp.int32, top.shape, 1)
    return jnp.where(lane < 64, pltpu.roll(top, 64, 1), bottom)


def slotted(rows, t):
    parts = rows.reshape(8, 1, 8, rows.shape[1])
    pair = [jnp.where(t == c, parts, 0.0) for c in range(2)]
    return jnp.concatenate(pair, axis=1).reshape(128, rows.shape[1])


def step(
    tok_h, state_h, gain_h, wq_h, wk_h, wd_h, wv_h, wg_h, off_h, hg_h, wo_h, mg_h, wu_h, wdn_h,
    mixed_ref, state,
    toks, unit, gain, wq, wk, wd, wv, wg, off, hg, mg, wo, wu, wdn,
    xg, wgat, zs, zr, ys, yr, cols, upright, vals, outs, gs, gr, gf, tokt, sp, sr, xf, wdt, part, fs, fr, fz, zr6, tw,
    send_sem, recv_sem, local_sem, gr_sem,
):
    kv, t = lax.axis_index("kv"), lax.axis_index("tp")
    y, z = lax.rem(kv, NY), lax.div(kv, NY)
    x = lax.axis_index("dp")
    other = 1 - t

    def at_x(dx):
        return lax.rem(x + dx, NX)

    def at_y(dy):
        return lax.rem(y + dy + NY, NY)

    def at_z(dz):
        return lax.rem(z + dz + NZ, NZ)

    barrier = pltpu.get_barrier_semaphore()

    def greet(to_y, to_z, to_t):
        pl.semaphore_signal(
            barrier, inc=1, device_id={"kv": to_z * NY + to_y, "tp": to_t}, device_id_type=MESH
        )

    greet(y, z, other)
    for dy in range(1, NY):
        greet(at_y(dy), z, t)
        greet(at_y(dy), z, other)
    for dz in range(1, NZ):
        greet(y, at_z(dz), t)
        greet(y, at_z(dz), other)
    for dx in range(1, NX):
        pl.semaphore_signal(barrier, inc=1, device_id={"dp": at_x(dx)}, device_id_type=MESH)
    greetings = 1 + 2 * (NY - 1) + 2 * (NZ - 1) + (NX - 1)

    local = []

    def fetch(src, dst):
        copy = pltpu.make_async_copy(src, dst, local_sem.at[len(local)])
        copy.start()
        local.append(copy)
        return copy

    sends = []

    def send(src, dst, to_y, to_z, to_t, recv=None, to_x=None):
        n = len(sends)
        to = {"kv": to_z * NY + to_y, "tp": to_t} if to_x is None else {"dp": to_x}
        copy = pltpu.make_async_remote_copy(
            src_ref=src,
            dst_ref=dst,
            send_sem=send_sem.at[n],
            recv_sem=recv_sem.at[n] if recv is None else recv,
            device_id=to,
            device_id_type=MESH,
        )
        copy.start()
        sends.append(copy)
        return copy

    drained = []

    def drain():
        for copy in sends[len(drained) :]:
            if copy is not None:
                copy.wait_send()
            drained.append(copy)

    tok_in = [fetch(tok_h, toks.at[t, z]), fetch(gain_h, gain)]
    weights, staged = (wq_h, wk_h, wd_h, wv_h, wg_h), (wq, wk, wd, wv, wg)
    weight_in, own_in = [None] * 5, [None] * 5
    for n in (3, 4, 0, 1, 2):
        weight_in[n] = fetch(weights[n], staged[n])
    for n in (3, 4, 0, 1, 2):
        width = COLUMNS[n].stop - COLUMNS[n].start
        mine = pl.ds(pl.multiple_of(y * width, width), width)
        own_in[n] = fetch(
            weights[n].at[:, mine], wgat.at[pl.ds(pl.multiple_of(y * 64, 64), 64), COLUMNS[n]]
        )
    half_lanes = pl.ds(pl.multiple_of(t * 128, 128), 128)
    half_rows = pl.ds(pl.multiple_of(t * 128, 128), 128)
    wo_in = fetch(wo_h, wo.at[t, z])
    wu_in = fetch(wu_h, wu.at[:, half_lanes])
    wdn_in = fetch(wdn_h, wdn.at[half_rows])
    small_in = [fetch(off_h, off), fetch(hg_h, hg), fetch(mg_h, mg)]
    state_in = fetch(state_h, state)

    for copy in tok_in:
        copy.wait()
    tok = toks[t, z].astype(F32)
    both_gains = jnp.broadcast_to(gain[...], (128, 64)).T
    my_gain = jnp.where(t == 0, both_gains[:32], both_gains[32:])
    squares = jnp.sum(tok * tok, axis=0, keepdims=True)
    high = squares.astype(BF16).astype(F32)
    rows = lax.broadcasted_iota(jnp.int32, (16, 128), 0)
    sums = jnp.where(rows == 0, high, jnp.where(rows == 1, squares - high, 0.0))
    unit[0:32] = (tok * my_gain).astype(BF16)
    unit[32:48] = sums.astype(BF16)
    xg[y, t] = unit[...]
    for copy in weight_in:
        copy.wait()

    pl.semaphore_wait(barrier, greetings)

    x_in = [send(unit, xg.at[y, t], y, z, other)]
    for dy in range(1, NY):
        x_in.append(send(unit, xg.at[y, t], at_y(dy), z, t))
        x_in.append(send(unit, xg.at[y, t], at_y(dy), z, other))
    w_in = [[] for _ in range(5)]
    for n in (3, 4, 0, 1, 2):
        width = COLUMNS[n].stop - COLUMNS[n].start
        for dy in (2, 1, 3):
            theirs = pl.ds(pl.multiple_of(at_y(dy) * width, width), width)
            w_in[n].append(
                send(
                    staged[n].at[:, theirs],
                    wgat.at[pl.ds(pl.multiple_of(y * 64, 64), 64), COLUMNS[n]],
                    at_y(dy),
                    z,
                    t,
                )
            )
    wo_in.wait()
    quarter = pl.ds(pl.multiple_of(x * 16, 16), 16)
    o_in = {}
    for dz in (1, 7, 2, 6, 3, 5, 4):
        o_in[dz] = send(wo.at[t, z, quarter], wo.at[t, z, quarter], y, at_z(dz), t)
    wu_in.wait()
    wdn_in.wait()
    twin_in = [
        send(wu.at[:, half_lanes], wu.at[:, half_lanes], y, z, other),
        send(wdn.at[half_rows], wdn.at[half_rows], y, z, other),
    ]
    q_in = []

    def hand_on(*hops):
        for dz in hops:
            o_in[dz].wait_recv()
            held = wo.at[t, at_z(-dz), quarter]
            for dx in (2, 1, 3):
                q_in.append(send(held, held, y, z, t, to_x=at_x(dx)))

    rows_of = (((1,), (1,)), ((), ()))
    for copy in x_in:
        copy.wait_recv()
    blocks = [xg[a, b].astype(F32) for a in range(NY) for b in range(2)]
    scaled = jnp.concatenate([block[0:32] for block in blocks], axis=0).T.astype(BF16)
    row_squares = sum(block[32:33] + block[33:34] for block in blocks)
    spread = jnp.broadcast_to(row_squares, (128, 128)).T
    spread_high = spread.astype(BF16).astype(F32)
    lane = lax.broadcasted_iota(jnp.int32, (128, 128), 1)
    zs[:, S] = jnp.where(lane < 64, spread_high, spread - spread_high).astype(BF16)
    hand_on(1, 7)
    z_in = []
    for columns, members in PIECES:
        for n in members:
            own_in[n].wait()
            for copy in w_in[n]:
                copy.wait_recv()
        if members == (2,):
            zs[:, R] = jnp.dot(scaled, wgat[:, R], preferred_element_type=F32).astype(BF16)
        else:
            zs[:, columns] = jnp.dot(scaled, wgat[:, columns], preferred_element_type=F32).astype(BF16)
        z_in.append([])
        for dz in (4, 3, 5, 2, 6, 1, 7):
            theirs = pl.ds(pl.multiple_of(at_z(dz) * 16, 16), 16)
            z_in[-1].append(
                send(zs.at[theirs, columns], zr.at[z, :, columns], y, at_z(dz), t)
            )
        if members == (3,):
            hand_on(2, 6)
    k_in = [send(toks.at[t, z], toks.at[t, z], y, at_z(dz), t) for dz in (4, 3, 5, 2, 6, 1, 7)]
    hand_on(3, 5, 4)
    for copy in twin_in:
        copy.wait_recv()
    for at in range(0, 2048, 256):
        wdt[at : at + 256] = wdn[:, at : at + 256].astype(F32).T.astype(BF16)
    for (columns, members), copies in zip(PIECES, z_in):
        mine = pl.ds(pl.multiple_of(z * 16, 16), 16)
        total = zs[mine, columns].astype(F32)
        for copy in copies:
            copy.wait_recv()
        for dz in range(1, NZ):
            total = total + zr[at_z(dz), :, columns].astype(F32)
        for a in range(NY):
            ys[a, :, columns] = total[4 * a : 4 * a + 4]
    y_in = [send(ys.at[at_y(dy)], yr.at[y], at_y(dy), z, t) for dy in (2, 1, 3)]
    yr[y] = ys[y]
    for copy in k_in + q_in:
        copy.wait_recv()
    twin_in = [
        send(wo.at[t], wo.at[t], y, z, other),
        send(toks.at[t], toks.at[t], y, z, other),
    ]
    for copy in small_in:
        copy.wait()
    state_in.wait()
    for copy in y_in:
        copy.wait_recv()

    got = [yr[a] for a in range(NY)]
    row_sum = got[0][:, 384:385] + got[0][:, 448:449]
    scale = lax.rsqrt(row_sum / D + EPS)
    queries = jnp.concatenate([g[:, Q] for g in got], axis=1) * scale * (256 ** -0.5)
    keys = jnp.concatenate([g[:, K] for g in got], axis=1) * scale
    retain = jax.nn.sigmoid(jnp.concatenate([g[:, R] for g in got], axis=1) * scale + off[...])
    cols[0:4] = queries * retain
    cols[4:8] = keys
    cols[8:12] = retain
    cols[12:16] = jnp.zeros((4, 512), F32)
    upright[...] = cols[...].T
    matches = queries * keys
    values = jnp.concatenate([g[:, V] for g in got], axis=1) * scale
    vals[...] = values
    gates = jnp.concatenate([g[:, G] for g in got], axis=1) * scale
    silu = gates * jax.nn.sigmoid(gates)
    for b in range(4):
        for h in range(2):
            total = jnp.zeros((8, 512), F32)
            for i in range(0, 256, 32):
                at = slice(h * 256 + i, h * 256 + i + 32)
                term = upright[at, b : b + 1] * state[b, h, i : i + 32, :]
                total = total + ((term[0:8] + term[8:16]) + (term[16:24] + term[24:32]))
            match = jnp.sum(matches[b : b + 1, h * 256 : h * 256 + 256], axis=1, keepdims=True)
            readout = (
                jnp.sum(total, axis=0, keepdims=True)
                + match * values[b : b + 1, h * 512 : h * 512 + 512]
            )
            power = jnp.mean(readout * readout, axis=1, keepdims=True)
            outs[b : b + 1, h * 512 : h * 512 + 512] = (
                readout * lax.rsqrt(power + EPS) * hg[...]
            )
    gs[...] = (outs[...] * silu).astype(BF16)

    low = lax.rem(y, 2)
    home = lax.div(y, 2)
    for dy in (2, 1, 3):
        send(gs, gr.at[low, t], at_y(dy), z, home, gr_sem.at[low, t])
    n = len(sends)

    @pl.when(home != t)
    def _():
        pltpu.make_async_remote_copy(
            src_ref=gs, dst_ref=gr.at[low, t], send_sem=send_sem.at[n], recv_sem=gr_sem.at[low, t],
            device_id={"kv": kv, "tp": other}, device_id_type=MESH,
        ).start()

    @pl.when(home == t)
    def _():
        gr[low, t] = gs[...]

    twin_gs = pltpu.make_async_copy(gs, gs, send_sem.at[n])
    sends.append(None)
    for b in range(4):
        for h in range(2):
            value = vals[b : b + 1, h * 512 : h * 512 + 512]
            for i in range(0, 256, 32):
                at = slice(h * 256 + i, h * 256 + i + 32)
                state[b, h, i : i + 32, :] = (
                    upright[at, 8 + b : 9 + b] * state[b, h, i : i + 32, :]
                    + upright[at, 4 + b : 5 + b] * value
                )
    drain()

    @pl.when(home != t)
    def _():
        twin_gs.wait()

    for copy in twin_in:
        copy.wait_recv()
    for p in range(4):
        own = jnp.concatenate([toks[c % 2, 2 * p + c // 2].astype(F32) for c in range(4)], axis=0)
        tokt[:, 128 * p : 128 * p + 128] = own.T
    here = pl.ds(pl.multiple_of(z * 16 + t * 8, 8), 8)
    own_tok = tokt[here]
    for a in range(2):
        for c in range(2):
            @pl.when(jnp.logical_or(y != 2 * t + a, t != c))
            def _():
                pltpu.make_async_copy(gs, gr.at[a, c], gr_sem.at[a, c]).wait()

            gf[4 * a : 4 * a + 4, 1024 * c : 1024 * c + 1024] = gr[a, c].astype(F32)

    gb = gf[...].astype(BF16)
    branch = sum(
        lax.dot_general(
            wo[c].reshape(512, 1024), gb[:, 1024 * c : 1024 * c + 1024], rows_of,
            preferred_element_type=F32,
        )
        for c in range(2)
    ).T
    sp[...] = (own_tok + branch).astype(BF16)
    s_in = {}
    for dz in (4, 3, 5, 2, 6, 1, 7):
        s_in[dz] = send(sp, sr.at[z, y], y, at_z(dz), t)
    sr[z, y] = sp[...]
    s_y = {}
    for dz in (0, 1, 7, 2, 6, 3, 5, 4):
        if dz:
            s_in[dz].wait_recv()
        src = at_z(-dz)
        s_y[dz] = [send(sr.at[src, y], sr.at[src, y], at_y(dy), z, t) for dy in (2, 1, 3)]
    drain()
    for dz in (0, 1, 7, 2, 6, 3, 5, 4):
        src = at_z(-dz)
        for copy in s_y[dz]:
            copy.wait_recv()
        rows = pl.ds(pl.multiple_of(src * 8, 8), 8)
        for p in range(2):
            for m in range(4):
                a = sr[src, 2 * p, :, 128 * m : 128 * m + 128].astype(F32)
                b = sr[src, 2 * p + 1, :, 128 * m : 128 * m + 128].astype(F32)
                at = 512 * m + 128 * p
                xf[rows, at : at + 128] = halves_side_by_side(a, b)
                xf[rows, at + 256 : at + 384] = second_halves(a, b)
    block = xf[...]
    power = jnp.sum(block * block, axis=1, keepdims=True)
    hidden = jnp.dot((block * mg[...]).astype(BF16), wu[...], preferred_element_type=F32)
    mlp_scale = lax.rsqrt(power / D + EPS)
    squared = slotted(jnp.square(jnp.maximum(hidden * mlp_scale, 0.0)), t).astype(BF16)
    near = pl.ds(pl.multiple_of(z * 256 + lax.div(y, 2) * 128, 128), 128)
    turned = slotted(xf[:, near], t).T
    turned = jnp.where(lax.rem(y, 2) == 0, turned[0:64], turned[64:128])
    own_stream = jnp.stack(
        [turned[c : c + 16] + pltpu.roll(turned[c + 16 : c + 32], 8, 1) for c in (0, 32)]
    )

    order = (4, 3, 5, 2, 6, 1, 7, 0)
    d_in = {}
    for dz in order:
        theirs = pl.ds(pl.multiple_of(at_z(dz) * 256, 256), 256)
        part[...] = lax.dot_general(wdt[theirs], squared, rows_of, preferred_element_type=F32)
        for a in range(NY):
            for c in range(2):
                at = 64 * a + 32 * c
                fs[dz, a, c] = (
                    part[at : at + 16] + pltpu.roll(part[at + 16 : at + 32], 8, 1)
                ).astype(BF16)
        d_in[dz] = [send(fs.at[dz, at_y(dy)], fr.at[dz, dy], at_y(dy), z, t) for dy in (2, 1, 3)]
    e_in = []
    for dz in order:
        for copy in d_in[dz]:
            copy.wait_recv()
        total = fs[dz, y].astype(F32)
        for dy in range(1, NY):
            total = total + fr[dz, dy].astype(F32)
        if dz:
            fz[dz] = total.astype(BF16)
            for c in (t, other):
                e_in.append(send(fz.at[dz, c], zr6.at[dz, t], y, at_z(dz), c))
    total = total + own_stream
    mine = jnp.where(t == 0, total[0], total[1])
    tw[0] = jnp.where(t == 0, total[1], total[0])
    tw_in = send(tw.at[0], tw.at[1], y, z, other)
    drain()
    for copy in e_in:
        copy.wait_recv()
    tw_in.wait_recv()
    theirs = tw[1]
    halves = [jnp.where(t == 0, mine, theirs), jnp.where(t == 0, theirs, mine)]
    for dz in range(1, NZ):
        halves = [halves[c] + zr6[dz, c].astype(F32) for c in range(2)]
    lane = lax.broadcasted_iota(jnp.int32, (16, 128), 1)
    first = lax.rem(lane, 16) < 8
    mixed_ref[0:16] = jnp.where(first, halves[0], halves[1]).astype(BF16)
    back = [pltpu.roll(half, 120, 1) for half in halves]
    mixed_ref[16:32] = jnp.where(first, back[0], back[1]).astype(BF16)
    drain()


def handed_on(mixed_in, new_in, mixed_ref, new_ref, sem):
    copies = [pltpu.make_async_copy(new_in.at[b], new_ref.at[b], sem.at[b]) for b in range(4)]
    copies.append(pltpu.make_async_copy(mixed_in, mixed_ref, sem.at[4]))
    for copy in copies:
        copy.start()
    for copy in copies:
        copy.wait()


SENDS = 7 + 15 + 7 + 2 + 21 + 28 + 7 + 3 + 2 + 4 + 7 + 24 + 24 + 14 + 1


def shards(tokens, state, mix_gain, w_query, w_key, w_decay, w_value, w_gate, decay_offset, head_gain, w_out, mlp_gain, w_up, w_down):
    anywhere = pl.BlockSpec(memory_space=pltpu.HBM)
    inside = pl.BlockSpec(memory_space=pltpu.VMEM)
    vmem = pltpu.VMEM
    mixed, new_state = pl.pallas_call(
        step,
        out_shape=(
            vmem(tokens.shape[::-1], BF16),
            vmem(state.shape, F32),
        ),
        in_specs=[anywhere] * 14,
        out_specs=(inside, inside),
        scratch_shapes=[
            vmem((2, 8, 32, 128), BF16),
            vmem((48, 128), BF16),
            vmem((1, 64), F32),
            vmem((64, 512), BF16),
            vmem((64, 512), BF16),
            vmem((64, 512), BF16),
            vmem((64, 1024), BF16),
            vmem((64, 1024), BF16),
            vmem((1, 512), F32),
            vmem((1, 512), F32),
            vmem((1, 2048), F32),
            vmem((2, 8, 64, 1024), BF16),
            vmem((2048, 256), BF16),
            vmem((256, 2048), BF16),
            vmem((4, 2, 48, 128), BF16),
            vmem((256, 1024), BF16),
            vmem((128, 1024), BF16),
            vmem((8, 16, 1024), BF16),
            vmem((4, 4, 1024), F32),
            vmem((4, 4, 1024), F32),
            vmem((16, 512), F32),
            vmem((512, 16), F32),
            vmem((4, 1024), F32),
            vmem((4, 1024), F32),
            vmem((4, 1024), BF16),
            vmem((2, 2, 4, 1024), BF16),
            vmem((8, 2048), F32),
            vmem((128, 512), F32),
            vmem((8, 512), BF16),
            vmem((8, 4, 8, 512), BF16),
            vmem((64, 2048), F32),
            vmem((2048, 256), BF16),
            vmem((256, 128), F32),
            vmem((8, 4, 2, 16, 128), BF16),
            vmem((8, 4, 2, 16, 128), BF16),
            vmem((8, 2, 16, 128), BF16),
            vmem((8, 2, 16, 128), BF16),
            vmem((2, 16, 128), F32),
            pltpu.SemaphoreType.DMA((SENDS,)),
            pltpu.SemaphoreType.DMA((SENDS,)),
            pltpu.SemaphoreType.DMA((32,)),
            pltpu.SemaphoreType.DMA((2, 2)),
        ],
        compiler_params=pltpu.CompilerParams(
            collective_id=0, has_side_effects=True, vmem_limit_bytes=62_500_000
        ),
        name="layer_step",
    )(
        tokens.T, state, mix_gain.reshape(1, -1), w_query, w_key, w_decay, w_value, w_gate,
        decay_offset.reshape(1, -1), head_gain.reshape(1, -1), w_out.T, mlp_gain.reshape(1, -1), w_up, w_down,
    )
    mixed, new_state = pl.pallas_call(
        handed_on,
        out_shape=(
            jax.ShapeDtypeStruct(mixed.shape, BF16),
            jax.ShapeDtypeStruct(state.shape, F32),
        ),
        in_specs=[inside] * 2,
        out_specs=(anywhere, anywhere),
        scratch_shapes=[pltpu.SemaphoreType.DMA((5,))],
        compiler_params=pltpu.CompilerParams(vmem_limit_bytes=1024 * 1024),
        name="handed_on",
    )(mixed, new_state)
    return mixed.T, new_state


def solution(mesh):
    in_specs = (
        P("dp", ("kv", "tp")),
        P(("dp", "kv"), "tp", None, None),
        P("kv"),
        P("kv", "tp"),
        P("kv", "tp"),
        P("kv", "tp"),
        P("kv", "tp"),
        P("kv", "tp"),
        P("tp"),
        P(),
        P("tp", "kv"),
        P(),
        P(None, ("kv", "tp")),
        P(("kv", "tp"), None),
    )
    out_specs = (P("dp", ("kv", "tp")), P(("dp", "kv"), "tp", None, None))
    return jax.shard_map(shards, mesh=mesh, in_specs=in_specs, out_specs=out_specs, check_vma=False)
```

time: 62.4 us -> 57.3 us (0.918)
  Pallas kernels: 61.6 us -> 56.5 us
    pallas_call x1, Pallas kernels: 59.6 us -> 54.4 us  [shards(): pl.pallas_call(step, out_shape=(vmem(tokens.shape[::-1], BF16), vmem(stat...]
where the time goes in v3:
time: 57.3 us; the launch traced here: 57.1 us
  Pallas kernels  56.5 us (99%)
  between operations  0.64 us (1%)
    pallas_call x1, Pallas kernels, shards(): pl.pallas_call(step, out_shape=(vmem(tokens.shape[::-1], BF16), vmem(stat...  54.4 us
    pallas_call x1, Pallas kernels, shards(): pl.pallas_call(handed_on, out_shape=(jax.ShapeDtypeStruct(mixed.shape, BF...  2.05 us

profile of v3, /device:TPU:1, one launch (start us, length us, event | category | flops | bytes accessed | tf_op | source)
XLA Modules:
  0.0 57.1 jit_solution(2945812430469806055)
XLA Ops:
  0.6 54.4 %layer_step.1 = (bf16[32,128]{1,0:T(8,128)(2,1)S(1)}, f32[4,2,256,512]{3,2,1,0:T(8,128)S(1)}) custom-call(bf16[32,128]{1,0:T(8,128)(2,1)} %bitcast.8, f32[4,2,256,512]{3,2,1,0:T(8,128)} %state_h.1, f32[1,64]{1,0:T(1,128)} %bitcast.12, bf16[64,512]{1,0:T(8,128)(2,1)} %wq_h.1, bf16[64,512]{1,0:T(8,128)(2,1)} %wk_h.1, bf16[64,512]{1,0:T(8,128)(2,1)} %wd_h.1, ...), custom_call_target="tpu_custom_call" | custom-call | tf_op jit(solution)/shard_map/layer_step/pallas_call | solution.py:424
  55.1 2.1 %handed_on.1 = (bf16[32,128]{1,0:T(8,128)(2,1)}, f32[4,2,256,512]{3,2,1,0:T(8,128)}) custom-call(bf16[32,128]{1,0:T(8,128)(2,1)S(1)} %get-tuple-element.6.mixed_in, f32[4,2,256,512]{3,2,1,0:T(8,128)S(1)} %get-tuple-element.7.new_in), custom_call_target="tpu_custom_call" | custom-call | tf_op jit(solution)/shard_map/handed_on/pallas_call | solution.py:484
